TPU v7x, 512 devices: a whole 4x4x16 slice. The times are simulated.
512 devices in a mesh: sp: 32 (over z, core), tp: 16 (over y, x).
Axes of the slice: x: 4, y: 4, z: 16, core: 2. Of those that a mesh axis runs over, the one named last changes fastest.
Arguments:
- residual: bfloat16 [8192, 2048], P('sp'), may hold values from -6 to 6
- queries: bfloat16 [8192, 16, 128], P('sp', 'tp'), may hold values from -256 to 256
- key_vectors: bfloat16 [8192, 16, 128], P('sp', 'tp'), may hold values from -5.3 to 5.3
- value_rows: bfloat16 [8192, 16, 128], P('sp', 'tp'), may hold values from -6 to 6
- head_lambda: float32 [16], P('tp'), may hold values from 0.3 to 0.8
- head_gain: float32 [128], replicated, may hold values from 0.1 to 1.9
- out_weight: bfloat16 [2048, 2048], P('tp'), may hold values from -0.125 to 0.125
- ffn_gain: float32 [2048], replicated, may hold values from 0.1 to 1.9
- expert_gate: bfloat16 [32, 2048, 4096], P('sp', None, 'tp'), may hold values from -0.125 to 0.125
- expert_up: bfloat16 [32, 2048, 4096], P('sp', None, 'tp'), may hold values from -0.125 to 0.125
- expert_down: bfloat16 [32, 4096, 2048], P('sp', None, 'tp'), may hold values from -0.09375 to 0.09375
- routing: int32 [8192, 2], P('sp'), may hold values from 0 to 31, as said below
- route_weight: float32 [8192, 2], P('sp'), may hold values from 0.1 to 0.9
Outputs:
- layer_out: bfloat16 [8192, 2048], P('sp')
Inputs may be any that keep to these rules, and one draw needn't show every extreme that they name: `routing`: each row names two different experts of one group of 8 consecutive experts. In each aligned block of 256 rows no expert is named by more than 32 rows, and in every block some expert is named by exactly 32 rows.
All inputs are finite; a program needn't handle non-finite values.
Results may differ from a plain program's by a relative error of at most 0.015.
Values may be sent and summed in bfloat16 or wider, within the bound.
No kernel may reach another device: no remote copies, remote signals or barrier semaphores. Data moves between devices by JAX's collectives and lax.ppermute only.
A program may use at most 64 MiB of HBM per device.

v0:
```python
import math
import jax
import jax.numpy as jnp
from jax import lax
from jax.sharding import PartitionSpec as P

GROUPS = 4
norm_eps = 1e-06


def sent_together(arrays, axis, dim, along):
    ends, at = ([], 0)
    for a in arrays[:-1]:
        at += a.shape[along]
        ends.append(at)
    both = jnp.concatenate(arrays, axis=along)
    return tuple(jnp.split(lax.all_gather(both, axis, axis=dim, tiled=True), ends, axis=along))


def in_blocks(array, dim, peers):
    before, after = (array.shape[:dim], array.shape[dim + 1 :])
    return jnp.moveaxis(array.reshape(*before, peers, -1, *after), dim, 0)


def sum_at_owner(array, axis, dim):
    parts = in_blocks(array, dim, lax.axis_size(axis))
    arrived = lax.all_to_all(parts, axis, split_axis=0, concat_axis=0, tiled=True)
    return arrived.astype(jnp.float32).sum(axis=0)


def padded_to(lines, peers):
    spare = -len(lines) % peers
    return jnp.pad(lines, [(0, spare)] + [(0, 0)] * (lines.ndim - 1))


def from_everyone(array, axis):
    peers = lax.axis_size(axis)
    return lax.all_to_all(
        jnp.broadcast_to(array[None], (peers, *array.shape)), axis, 0, 0, tiled=True
    )


def laid_out(parts, dim):
    parts = jnp.moveaxis(parts, 0, dim)
    dims = parts.shape
    return parts.reshape(*dims[:dim], dims[dim] * dims[dim + 1], *dims[dim + 2 :])


def collect(array, axis, dim):
    parts = from_everyone(array, axis)
    return laid_out(parts, dim)


def sum_by_parts(array, axes):
    lines = array.reshape(-1, array.shape[-1])
    own = sum_at_owner(padded_to(lines, lax.axis_size(axes)), axes, 0)
    whole = collect(own.astype(jnp.bfloat16), axes, 0)
    return whole[: len(lines)].reshape(array.shape).astype(jnp.float32)


def online_update(running, query_part, key_part, value_part, query_pos, key_pos, score_scale):
    highest, totals, accum = running
    scores = (
        jnp.einsum("qhd,khd->hqk", query_part, key_part, preferred_element_type=jnp.float32)
        * score_scale
    )
    scores = jnp.where(key_pos[None, None, :] <= query_pos[None, :, None], scores, -jnp.inf)
    new_high = jnp.maximum(highest, jnp.max(scores, axis=-1))
    shrink = jnp.exp(highest - new_high)
    weights = jnp.exp(scores - new_high[:, :, None])
    totals = shrink * totals + jnp.sum(weights, axis=-1)
    blended = jnp.einsum(
        "hqk,khe->qhe", weights.astype(jnp.bfloat16), value_part, preferred_element_type=jnp.float32
    )
    accum = jnp.transpose(shrink)[:, :, None] * accum + blended
    return (new_high, totals, accum)


def shards(
    residual,
    queries,
    key_vectors,
    value_rows,
    head_lambda,
    head_gain,
    out_weight,
    ffn_gain,
    expert_gate,
    expert_up,
    expert_down,
    routing,
    route_weight,
):
    tok_count = queries.shape[0]
    local_heads = queries.shape[1]
    half_width = queries.shape[2] // 2
    value_width = value_rows.shape[2]
    score_scale = half_width ** (-0.5)
    query_pos = lax.axis_index("sp") * tok_count + jnp.arange(tok_count, dtype=jnp.int32)
    last_query = query_pos[-1]
    first_half = queries[:, :, :half_width]
    second_half = queries[:, :, half_width:]
    start_high = jnp.full((local_heads, tok_count), -1e30, jnp.float32)
    start_total = jnp.zeros((local_heads, tok_count), jnp.float32)
    start_accum = jnp.zeros((tok_count, local_heads, value_width), jnp.float32)
    empty_state = (start_high, start_total, start_accum)
    running = (empty_state, empty_state)
    key_piece, value_piece = sent_together((key_vectors, value_rows), "sp", 0, 1)
    piece_len = key_piece.shape[0]
    block_len = math.gcd(piece_len, 512)
    block_count = piece_len // block_len
    key_blocks = key_piece.reshape(block_count, block_len, local_heads, 2 * half_width)
    value_blocks = value_piece.reshape(block_count, block_len, local_heads, value_width)

    def visit(current, stacked):
        block_index, key_block, value_block = stacked
        block_first = block_index * block_len
        key_pos = block_first + jnp.arange(block_len, dtype=jnp.int32)

        def compute(inside):
            first_state = online_update(
                inside[0],
                first_half,
                key_block[:, :, :half_width],
                value_block,
                query_pos,
                key_pos,
                score_scale,
            )
            second_state = online_update(
                inside[1],
                second_half,
                key_block[:, :, half_width:],
                value_block,
                query_pos,
                key_pos,
                score_scale,
            )
            return (first_state, second_state)

        return (lax.cond(block_first <= last_query, compute, lambda inside: inside, current), None)

    running, _ = lax.scan(
        visit, running, (jnp.arange(block_count, dtype=jnp.int32), key_blocks, value_blocks)
    )
    first_state, second_state = running
    first_out = first_state[2] / jnp.transpose(first_state[1])[:, :, None]
    second_out = second_state[2] / jnp.transpose(second_state[1])[:, :, None]
    combined = first_out - head_lambda[None, :, None] * second_out
    normed_heads = (
        combined
        * lax.rsqrt(jnp.mean(combined * combined, axis=-1, keepdims=True) + norm_eps)
        * head_gain
    )
    attended = normed_heads.astype(jnp.bfloat16).reshape(tok_count, local_heads * value_width)
    partial_proj = jnp.dot(attended, out_weight, preferred_element_type=jnp.float32)
    projected = sum_by_parts(partial_proj.astype(jnp.bfloat16), "tp")
    stream = residual.astype(jnp.float32) + projected
    block_normed = (
        stream * lax.rsqrt(jnp.mean(stream * stream, axis=-1, keepdims=True) + norm_eps) * ffn_gain
    ).astype(jnp.bfloat16)
    expert_count = lax.axis_size("sp")
    tp_count = lax.axis_size("tp")
    per_group = expert_count // GROUPS
    capacity = tok_count // per_group
    top_count = routing.shape[1]
    model_width = block_normed.shape[1]
    flat_routes = routing.reshape(-1)
    route_count = flat_routes.shape[0]
    onehot = (flat_routes[:, None] == jnp.arange(expert_count, dtype=jnp.int32)[None, :]).astype(
        jnp.int32
    )
    earlier = jnp.cumsum(onehot, axis=0) - onehot
    position = jnp.sum(earlier * onehot, axis=1)
    slot_index = flat_routes * capacity + position
    slot_token = (
        jnp.full((expert_count * capacity,), tok_count, jnp.int32)
        .at[slot_index]
        .set(jnp.arange(route_count, dtype=jnp.int32) // top_count)
    )
    slot_table = slot_token.reshape(expert_count, capacity)
    slice_width = model_width // tp_count
    own_columns = lax.dynamic_slice_in_dim(
        block_normed, lax.axis_index("tp") * slice_width, slice_width, 1
    )
    outgoing = jnp.take(own_columns, slot_table, axis=0, mode="fill", fill_value=0)
    landed = lax.all_to_all(outgoing, "sp", split_axis=0, concat_axis=0, tiled=True)
    arrived = collect(landed, "tp", 2)
    expert_rows = arrived.reshape(-1, model_width)
    gate_part = jnp.dot(expert_rows, expert_gate[0], preferred_element_type=jnp.float32)
    up_part = jnp.dot(expert_rows, expert_up[0], preferred_element_type=jnp.float32)
    inner_act = (jax.nn.silu(gate_part) * up_part).astype(jnp.bfloat16)
    down_width = expert_down.shape[2]
    weight_rows = expert_down[0]
    expert_sum = jnp.dot(
        lax.all_gather(inner_act, "tp", axis=1, tiled=True),
        weight_rows,
        preferred_element_type=jnp.float32,
    )
    expert_out = expert_sum.astype(jnp.bfloat16).reshape(expert_count, capacity, down_width)
    returned = lax.all_to_all(expert_out, "sp", split_axis=0, concat_axis=0, tiled=True)
    per_route = returned.reshape(expert_count * capacity, down_width)[slot_index]
    weighted = per_route.astype(jnp.float32) * route_weight.reshape(-1)[:, None]
    token_sum = jnp.sum(weighted.reshape(tok_count, top_count, down_width), axis=1)
    moe_rows = collect(token_sum.astype(jnp.bfloat16), "tp", 1).astype(token_sum.dtype)
    return (stream + moe_rows).astype(jnp.bfloat16)


def solution(mesh):
    in_specs = (
        P("sp", None),
        P("sp", "tp", None),
        P("sp", "tp", None),
        P("sp", "tp", None),
        P("tp"),
        P(),
        P("tp", None),
        P(),
        P("sp", None, "tp"),
        P("sp", None, "tp"),
        P("sp", None, "tp"),
        P("sp", None),
        P("sp", None),
    )
    out_specs = P("sp", None)
    return jax.shard_map(shards, mesh=mesh, in_specs=in_specs, out_specs=out_specs, check_vma=False)
```

profile of v0, /device:TPU:1, one launch (start us, length us, event | category | flops | bytes accessed | tf_op | source)
XLA Modules:
  0.0 460.8 jit_solution(17257785034887943455)
XLA Ops:
  6.5 1.6 pad_maximum_fusion
  8.2 0.6 slice.25
  8.9 1.0 fusion.59
  10.7 78.0 %all-gather.3.cloned.1.call-done = bf16[8192,2,128]{2,0,1:T(8,128)(2,1)} async-done(((bf16[256,2,128]{2,0,1:T(8,128)(2,1)}), bf16[8192,2,128]{2,0,1:T(8,128)(2,1)}) %all-gather.3.cloned.1.call-update) | async-done | bytes 4194320 | tf_op jit(solution)/shard_map/all_gather | solution.py:17
  88.7 3.8 fusion.58
  92.6 33.3 %while.21 = (s32[]{:T(128)}, f32[1,256]{1,0:T(1,128)S(1)}, f32[1,256]{1,0:T(1,128)S(1)}, f32[256,1,128]{0,2,1:T(8,128)S(1)}, f32[1,256]{1,0:T(1,128)S(1)}, /*ind...) while((s32[]{:T(128)}, f32[1,256]{1,0:T(1,128)S(1)}, ...), condition=%wide.region_7.8_spmd.clone, body=%wide.region_0.7_spmd.clone.sunk | while | flops 102893312 | bytes 4570543 | solution.py:143
  92.6 0.6 dynamic_slice.42
  94.5 2.4 conditional.3
  94.5 0.9 dynamic-slice_bitcast_fusion
  95.5 0.2 fusion.56
  95.8 0.1 fusion.9
  95.9 0.3 fusion.57
  96.3 0.3 fusion.7
  96.6 0.3 fusion.6
  97.0 0.6 dynamic_slice.42
  98.9 0.6 dynamic_slice.42
  100.8 0.6 dynamic_slice.42
  102.8 0.6 dynamic_slice.42
  104.7 0.6 dynamic_slice.42
  106.6 0.6 dynamic_slice.42
  108.6 0.6 dynamic_slice.42
  110.5 0.6 dynamic_slice.42
  112.4 0.6 dynamic_slice.42
  114.4 0.6 dynamic_slice.42
  116.3 0.6 dynamic_slice.42
  118.2 0.6 dynamic_slice.42
  120.2 0.6 dynamic_slice.42
  122.1 0.6 dynamic_slice.42
  124.0 0.6 dynamic_slice.42
  126.0 2.5 convolution_convert_fusion
  128.6 6.5 %all-to-all-start = ((bf16[16,16,2048]{2,1,0:T(8,128)(2,1)}), bf16[16,16,2048]{2,1,0:T(8,128)(2,1)S(1)}, u32[]{:S(2)}, u32[]{:S(2)}) async-start(bf16[16,16,2048]{2,1,0:T(8,128)(2,1)} %bitcast.29), calls=%async_computation | async-start | bytes 2097152 | tf_op jit(solution)/shard_map/all_to_all | solution.py:27
  135.1 0.1 copy.31
  135.3 0.1 eq.29
  135.4 0.1 eq.25
  135.6 1.2 reduce-window.6
  136.7 0.2 slice_reduce_fusion
  137.0 0.1 copy.30
  137.2 0.1 mul.162
  137.4 14.1 %all-to-all-done = bf16[16,16,2048]{2,1,0:T(8,128)(2,1)S(1)} async-done(((bf16[16,16,2048]{2,1,0:T(8,128)(2,1)}), bf16[16,16,2048]{2,1,0:T(8,128)(2,1)S(1)}, u32[]{:S(2)}, u32[]{:S(2)}) %all-to-all-start) | async-done | bytes 1048608 | tf_op jit(solution)/shard_map/all_to_all | solution.py:27
  151.5 0.1 reduce_sum.73
  151.7 1.1 broadcast_in_dim.38
  152.8 4.5 all-to-all-start.1
  157.4 2.4 scatter_custom_fusion
  160.0 0.8 dynamic-slice
  160.8 12.4 %all-to-all-done.1 = bf16[16,16,2048]{2,1,0:T(8,128)(2,1)S(1)} async-done(((bf16[16,16,2048]{2,1,0:T(8,128)(2,1)}), bf16[16,16,2048]{2,1,0:T(8,128)(2,1)S(1)}, u32[]{:S(2)}, u32[]{:S(2)}) %all-to-all-start.1) | async-done | bytes 1048608 | tf_op jit(solution)/shard_map/all_to_all | solution.py:38
  173.2 0.4 multiply_reduce_fusion
  173.7 3.2 gather_fusion
  176.9 0.2 broadcast_select_fusion
  177.2 65.0 %all_to_all.30 = bf16[32,32,128]{2,1,0:T(8,128)(2,1)S(1)} all-to-all(bf16[32,32,128]{2,1,0:T(8,128)(2,1)S(1)} %broadcast_select_fusion), channel_id=1, replica_groups=mesh['sp'=32,'tp'=16] {'sp'}, dimensions={0} | all-to-all | bytes 524288 | tf_op jit(solution)/shard_map/all_to_all | solution.py:187
  242.1 0.8 broadcast_in_dim.42
  242.9 52.7 %all_to_all.31 = bf16[16,32,32,128]{3,2,1,0:T(8,128)(2,1)S(1)} all-to-all(bf16[16,32,32,128]{3,2,1,0:T(8,128)(2,1)S(1)} %broadcast_in_dim.42), channel_id=1, replica_groups=mesh['sp'=32,'tp'=16] {'tp'}, dimensions={0} | all-to-all | bytes 8388608 | tf_op jit(solution)/shard_map/all_to_all | solution.py:38
  295.6 4.9 %copy.34 = bf16[32,32,16,128]{3,2,1,0:T(8,128)(2,1)S(1)} copy(bf16[32,32,16,128]{3,1,0,2:T(8,128)(2,1)S(1)} %bitcast.139) | data formatting | bytes 8388608 | tf_op jit(solution)/shard_map/transpose | solution.py:44
  300.5 1.3 fusion.26
  301.8 2.1 fusion.34
  303.9 81.9 %all-gather.5.cloned.1.call-done = bf16[1024,4096]{1,0:T(8,128)(2,1)} async-done(((bf16[1024,256]{1,0:T(8,128)(2,1)}), bf16[1024,4096]{1,0:T(8,128)(2,1)}) %all-gather.5.cloned.1.call-update) | async-done | bytes 8388624 | tf_op jit(solution)/shard_map/all_gather | solution.py:196
  385.8 6.6 %convolution_convert_fusion.1 = bf16[1024,128]{1,0:T(8,128)(2,1)} fusion(bf16[1024,4096]{1,0:T(8,128)(2,1)} %all-gather.5.cloned.1.call-done, bf16[1,4096,128]{2,1,0:T(8,128)(2,1)} %param.27), kind=kOutput, calls=%fused_computation.53 | convolution fusion | flops 1073872896 | bytes 9699328 | tf_op jit(solution)/shard_map/dot_general | solution.py:195
  392.4 14.4 %all-to-all-start.4 = ((bf16[32,32,128]{2,1,0:T(8,128)(2,1)}), bf16[32,32,128]{2,1,0:T(8,128)(2,1)S(1)}, u32[]{:S(2)}, u32[]{:S(2)}) async-start(bf16[32,32,128]{2,1,0:T(8,128)(2,1)} %bitcast.151), calls=%async_computation.4 | async-start | bytes 524288 | tf_op jit(solution)/shard_map/all_to_all | solution.py:201
  406.8 0.8 copy.35
  407.6 21.5 %all-to-all-done.4 = bf16[32,32,128]{2,1,0:T(8,128)(2,1)S(1)} async-done(((bf16[32,32,128]{2,1,0:T(8,128)(2,1)}), bf16[32,32,128]{2,1,0:T(8,128)(2,1)S(1)}, u32[]{:S(2)}, u32[]{:S(2)}) %all-to-all-start.4) | async-done | bytes 262176 | tf_op jit(solution)/shard_map/all_to_all | solution.py:201
  429.1 1.3 gather_fusion.1
  430.4 1.3 fusion.40
  431.8 0.2 broadcast_in_dim.43
  432.0 20.5 %all_to_all.32 = bf16[16,256,128]{2,1,0:T(8,128)(2,1)S(1)} all-to-all(bf16[16,256,128]{2,1,0:T(8,128)(2,1)S(1)} %broadcast_in_dim.43), channel_id=1, replica_groups=mesh['sp'=32,'tp'=16] {'tp'}, dimensions={0} | all-to-all | bytes 2097152 | tf_op jit(solution)/shard_map/all_to_all | solution.py:38
  452.5 1.5 fusion.30
  (99 shorter events, 1.4 us)
Async XLA Ops:
  6.5 294.0 %copy-start = (bf16[1,2048,256]{2,1,0:T(8,128)(2,1)S(1)}, bf16[1,2048,256]{2,1,0:T(8,128)(2,1)}, u32[]{:S(2)}) copy-start(bf16[1,2048,256]{2,1,0:T(8,128)(2,1)} %param.25) | copy-start | bytes 3145732
  6.5 82.2 %all-gather.3.cloned.1.call-start = ((), (), s32[]{:S(2)}) async-start(), calls=%async_computation.6 | async-start | bytes 4325376 | tf_op jit(solution)/shard_map/all_gather | solution.py:17
  92.6 33.4 %copy-start.4 = (f32[128]{0:T(128)S(1)}, f32[128]{0:T(128)}, u32[]{:S(2)}) copy-start(f32[128]{0:T(128)} %param.22) | copy-start | bytes 1540
  126.0 9.2 %copy-start.2 = (s32[256,2]{0,1:T(2,128)S(1)}, s32[256,2]{0,1:T(2,128)}, u32[]{:S(2)}) copy-start(s32[256,2]{0,1:T(2,128)} %param.28) | copy-start | bytes 6148
  128.6 23.0 %all-to-all-start = ((bf16[16,16,2048]{2,1,0:T(8,128)(2,1)}), bf16[16,16,2048]{2,1,0:T(8,128)(2,1)S(1)}, u32[]{:S(2)}, u32[]{:S(2)}) async-start(bf16[16,16,2048]{2,1,0:T(8,128)(2,1)} %bitcast.29), calls=%async_computation | async-start | bytes 2097152 | tf_op jit(solution)/shard_map/all_to_all | solution.py:27
  137.4 35.8 %copy-start.1 = (bf16[256,2048]{1,0:T(8,128)(2,1)S(1)}, bf16[256,2048]{1,0:T(8,128)(2,1)}, u32[]{:S(2)}) copy-start(bf16[256,2048]{1,0:T(8,128)(2,1)} %param.17) | copy-start | bytes 3145732
  152.8 20.4 %all-to-all-start.1 = ((bf16[16,16,2048]{2,1,0:T(8,128)(2,1)}), bf16[16,16,2048]{2,1,0:T(8,128)(2,1)S(1)}, u32[]{:S(2)}, u32[]{:S(2)}) async-start(bf16[16,16,2048]{2,1,0:T(8,128)(2,1)} %broadcast_in_dim.38), calls=%async_computation.1 | async-start | bytes 2097152 | tf_op jit(solution)/shard_map/all_to_all | solution.py:38
  157.3 228.5 %all-gather.5.cloned.1.call-start = ((), (), s32[]{:S(2)}) async-start(), calls=%async_computation.7 | async-start | bytes 8912896 | tf_op jit(solution)/shard_map/all_gather | solution.py:196
  300.5 1.3 copy-start.5
  303.9 102.9 %copy-start.3 = (f32[256,2]{0,1:T(2,128)S(1)}, f32[256,2]{0,1:T(2,128)}, u32[]{:S(2)}) copy-start(f32[256,2]{0,1:T(2,128)} %param.29) | copy-start | bytes 6148
  392.4 36.6 %all-to-all-start.4 = ((bf16[32,32,128]{2,1,0:T(8,128)(2,1)}), bf16[32,32,128]{2,1,0:T(8,128)(2,1)S(1)}, u32[]{:S(2)}, u32[]{:S(2)}) async-start(bf16[32,32,128]{2,1,0:T(8,128)(2,1)} %bitcast.151), calls=%async_computation.4 | async-start | bytes 524288 | tf_op jit(solution)/shard_map/all_to_all | solution.py:201
Sparse Core Ops, SparseCore 0:
  9.5 79.1 all-gather.2
  304.0 81.7 all-gather.4
where the time goes:
time: 462 us; the launch traced here: 461 us
  waiting for transfers between devices  208 us (45%)
  blocking collectives  138 us (30%)
  local copies, waits for them, and re-layouts  32.7 us (7%)
  starting transfers between devices  25.4 us (5%)
  loops' own time  21.5 us (5%)
  between operations  14.4 us (3%)
  matrix products  13.6 us (3%)
  other arithmetic  7.04 us (2%)
    all_gather x1, waiting for transfers between devices, shards(): lax.all_gather(inner_act, 'tp', axis=1, tiled=True)  81.9 us
    all_gather x1, waiting for transfers between devices, sent_together(): lax.all_gather(both, axis, axis=dim, tiled=True)  78 us
    all_to_all x2, blocking collectives, from_everyone(): lax.all_to_all(jnp.broadcast_to(array[None], (peers, *array.shape)), axis...  73.2 us
    all_to_all x1, blocking collectives, shards(): lax.all_to_all(outgoing, 'sp', split_axis=0, concat_axis=0, tiled=True)  65 us
    all_to_all x1, waiting for transfers between devices, shards(): lax.all_to_all(expert_out, 'sp', split_axis=0, concat_axis=0, tiled=True)  21.5 us
    another operation x1, loops' own time, shards(): lax.scan(visit, running, (jnp.arange(block_count, dtype=jnp.int32), key_b...  21.2 us
    all_to_all x1, starting transfers between devices, shards(): lax.all_to_all(expert_out, 'sp', split_axis=0, concat_axis=0, tiled=True)  14.4 us
    all_to_all x1, waiting for transfers between devices, sum_at_owner(): lax.all_to_all(parts, axis, split_axis=0, concat_axis=0, tiled=True)  14.1 us
  transfers between devices with their start and end apart: 5, of which 5 were waited for; matrix products, arithmetic and copies ran while one was open for 2% of the time, Pallas kernels for 0%

commit v1 on v0

--- a/solution.py
+++ b/solution.py
@@ -6,6 +6,22 @@
 
 GROUPS = 4
 norm_eps = 1e-06
+
+
+def ring_gather(x, axis, dim):
+    ways, here, step = (lax.axis_size(axis), lax.axis_index(axis), x.shape[dim])
+    lengths = [n * ways if d == dim else n for d, n in enumerate(x.shape)]
+    full = lax.dynamic_update_slice_in_dim(jnp.zeros(lengths, x.dtype), x, here * step, axis=dim)
+    going_up = going_down = x
+    for far in range(1, ways // 2 + 1):
+        going_up = lax.ppermute(going_up, axis, [(d, (d + 1) % ways) for d in range(ways)])
+        full = lax.dynamic_update_slice_in_dim(full, going_up, (here - far) % ways * step, axis=dim)
+        if 2 * far < ways:
+            going_down = lax.ppermute(going_down, axis, [(d, (d - 1) % ways) for d in range(ways)])
+            full = lax.dynamic_update_slice_in_dim(
+                full, going_down, (here + far) % ways * step, axis=dim
+            )
+    return full
 
 
 def sent_together(arrays, axis, dim, along):
@@ -193,9 +209,7 @@
     down_width = expert_down.shape[2]
     weight_rows = expert_down[0]
     expert_sum = jnp.dot(
-        lax.all_gather(inner_act, "tp", axis=1, tiled=True),
-        weight_rows,
-        preferred_element_type=jnp.float32,
+        ring_gather(inner_act, "tp", 1), weight_rows, preferred_element_type=jnp.float32
     )
     expert_out = expert_sum.astype(jnp.bfloat16).reshape(expert_count, capacity, down_width)
     returned = lax.all_to_all(expert_out, "sp", split_axis=0, concat_axis=0, tiled=True)

time: 462 us -> 534 us (1.16)
  starting transfers between devices: 25.4 us -> 96 us
  blocking collectives: 138 us -> 84 us
  local copies, waits for them, and re-layouts: 32.7 us -> 67.5 us
  waiting for transfers between devices: 208 us -> 228 us
    all_gather x1 -> x0, waiting for transfers between devices: 81.9 us -> none  [shards(): lax.all_gather(inner_act, 'tp', axis=1, tiled=True)]
    all_to_all x1 -> x2, waiting for transfers between devices: 12.4 us -> 74.9 us  [from_everyone(): lax.all_to_all(jnp.broadcast_to(array[None], (peers, *array.shape)), axis...]
    ppermute x0 -> x15, starting transfers between devices: none -> 62.3 us  [the longest x7 46.8 us: ring_gather(): lax.ppermute(going_down, axis, [(d, (d - 1) % ways) for d in range(ways)])]
    all_to_all x2 -> x1, blocking collectives: 73.2 us -> 19 us  [from_everyone(): lax.all_to_all(jnp.broadcast_to(array[None], (peers, *array.shape)), axis...]
    ppermute x0 -> x15, waiting for transfers between devices: none -> 39 us  [the longest x8 39 us: ring_gather(): lax.ppermute(going_up, axis, [(d, (d + 1) % ways) for d in range(ways)])]
    dynamic_update_slice x0 -> x15, local copies, waits for them, and re-layouts: none -> 24.8 us  [the longest x8 13.4 us: ring_gather(): lax.dynamic_update_slice_in_dim(full, going_up, (here - far) % ways * ste...]
  transfers between devices with their start and end apart: 5 -> 20, of which waited for: 5 -> 11; matrix products, arithmetic and copies ran while one was open for 2% -> 6% of each run, Pallas kernels for 0% -> 0%
where the time goes in v1:
time: 534 us; the launch traced here: 532 us
  waiting for transfers between devices  228 us (43%)
  starting transfers between devices  96 us (18%)
  blocking collectives  84 us (16%)
  local copies, waits for them, and re-layouts  67.5 us (13%)
  loops' own time  21.3 us (4%)
  between operations  14.8 us (3%)
  matrix products  13.6 us (3%)
  other arithmetic  7.1 us (1%)
    all_gather x1, waiting for transfers between devices, sent_together(): lax.all_gather(both, axis, axis=dim, tiled=True)  78 us
    all_to_all x2, waiting for transfers between devices, from_everyone(): lax.all_to_all(jnp.broadcast_to(array[None], (peers, *array.shape)), axis...  74.9 us
    all_to_all x1, blocking collectives, shards(): lax.all_to_all(outgoing, 'sp', split_axis=0, concat_axis=0, tiled=True)  65 us
    ppermute x7, starting transfers between devices, ring_gather(): lax.ppermute(going_down, axis, [(d, (d - 1) % ways) for d in range(ways)])  46.8 us
    ppermute x8, waiting for transfers between devices, ring_gather(): lax.ppermute(going_up, axis, [(d, (d + 1) % ways) for d in range(ways)])  39 us
    all_to_all x1, waiting for transfers between devices, shards(): lax.all_to_all(expert_out, 'sp', split_axis=0, concat_axis=0, tiled=True)  21.4 us
    another operation x1, loops' own time, shards(): lax.scan(visit, running, (jnp.arange(block_count, dtype=jnp.int32), key_b...  21 us
    all_to_all x1, blocking collectives, from_everyone(): lax.all_to_all(jnp.broadcast_to(array[None], (peers, *array.shape)), axis...  19 us
  transfers between devices with their start and end apart: 20, of which 11 were waited for; matrix products, arithmetic and copies ran while one was open for 6% of the time, Pallas kernels for 0%

profile of v1, /device:TPU:1, one launch (start us, length us, event | category | flops | bytes accessed | tf_op | source)
XLA Modules:
  0.0 531.8 jit_solution(4245987626586289316)
XLA Ops:
  6.5 1.6 pad_maximum_fusion
  8.9 1.0 fusion.59
  10.7 78.0 %all-gather.2.cloned.1.call-done = bf16[8192,2,128]{2,0,1:T(8,128)(2,1)} async-done(((bf16[256,2,128]{2,0,1:T(8,128)(2,1)}), bf16[8192,2,128]{2,0,1:T(8,128)(2,1)}) %all-gather.2.cloned.1.call-update) | async-done | bytes 4194320 | tf_op jit(solution)/shard_map/all_gather | solution.py:33
  88.7 3.8 fusion.58
  92.6 33.1 %while.21 = (s32[]{:T(128)}, f32[1,256]{1,0:T(1,128)S(1)}, f32[1,256]{1,0:T(1,128)S(1)}, f32[256,1,128]{0,2,1:T(8,128)S(1)}, f32[1,256]{1,0:T(1,128)S(1)}, /*ind...) while((s32[]{:T(128)}, f32[1,256]{1,0:T(1,128)S(1)}, ...), condition=%wide.region_7.8_spmd.clone, body=%wide.region_0.7_spmd.clone.sunk | while | flops 102893312 | bytes 4570543 | solution.py:159
  94.5 2.4 conditional.3
  94.6 0.9 dynamic-slice_bitcast_fusion
  125.9 2.6 convolution_convert_fusion
  128.5 6.5 %all-to-all-start = ((bf16[16,16,2048]{2,1,0:T(8,128)(2,1)}), bf16[16,16,2048]{2,1,0:T(8,128)(2,1)S(1)}, u32[]{:S(2)}, u32[]{:S(2)}) async-start(bf16[16,16,2048]{2,1,0:T(8,128)(2,1)} %bitcast.147), calls=%async_computation | async-start | bytes 2097152 | tf_op jit(solution)/shard_map/all_to_all | solution.py:43
  135.5 1.2 reduce-window.6
  137.3 14.1 %all-to-all-done = bf16[16,16,2048]{2,1,0:T(8,128)(2,1)S(1)} async-done(((bf16[16,16,2048]{2,1,0:T(8,128)(2,1)}), bf16[16,16,2048]{2,1,0:T(8,128)(2,1)S(1)}, u32[]{:S(2)}, u32[]{:S(2)}) %all-to-all-start) | async-done | bytes 1048608 | tf_op jit(solution)/shard_map/all_to_all | solution.py:43
  151.6 1.1 broadcast_in_dim.40
  152.7 4.5 all-to-all-start.1
  157.2 2.4 scatter_custom_fusion
  160.7 12.4 %all-to-all-done.1 = bf16[16,16,2048]{2,1,0:T(8,128)(2,1)S(1)} async-done(((bf16[16,16,2048]{2,1,0:T(8,128)(2,1)}), bf16[16,16,2048]{2,1,0:T(8,128)(2,1)S(1)}, u32[]{:S(2)}, u32[]{:S(2)}) %all-to-all-start.1) | async-done | bytes 1048608 | tf_op jit(solution)/shard_map/all_to_all | solution.py:54
  173.6 3.2 gather_fusion
  177.0 65.0 %all_to_all.30 = bf16[32,32,128]{2,1,0:T(8,128)(2,1)S(1)} all-to-all(bf16[32,32,128]{2,1,0:T(8,128)(2,1)S(1)} %broadcast_select_fusion), channel_id=1, replica_groups=mesh['sp'=32,'tp'=16] {'sp'}, dimensions={0} | all-to-all | bytes 524288 | tf_op jit(solution)/shard_map/all_to_all | solution.py:203
  242.0 2.8 broadcast_in_dim.70
  244.8 4.7 all-to-all-start.3
  249.6 62.5 %all-to-all-done.3 = bf16[16,32,32,128]{3,2,1,0:T(8,128)(2,1)} async-done(((bf16[16,32,32,128]{3,2,1,0:T(8,128)(2,1)}), bf16[16,32,32,128]{3,2,1,0:T(8,128)(2,1)}, u32[]{:S(2)}, u32[]{:S(2)}) %all-to-all-start.3) | async-done | bytes 4194336 | tf_op jit(solution)/shard_map/all_to_all | solution.py:54
  312.1 7.1 %copy.34 = bf16[32,32,16,128]{3,2,1,0:T(8,128)(2,1)S(1)} copy(bf16[32,32,16,128]{3,1,0,2:T(8,128)(2,1)} %bitcast.35) | data formatting | bytes 8388608 | tf_op jit(solution)/shard_map/transpose | solution.py:60
  319.2 1.3 fusion.26
  320.5 4.3 broadcast_in_dim.41
  324.8 2.2 constant_dynamic-update-slice_fusion.15
  326.9 1.9 collective-permute-start
  328.8 6.7 %collective-permute-start.1 = (bf16[1024,256]{1,0:T(8,128)(2,1)S(1)}, bf16[1024,256]{1,0:T(8,128)(2,1)S(1)}, u32[]{:S(2)}, u32[]{:S(2)}) collective-permute-start(bf16[1024,256]{1,0:T(8,128)(2,1)S(1)} %get-tuple-element.328), channel_id=1, source_target_pairs={{0,15},{1,0},{2,1},{3,2},{4,3},{5,4},{6,5},{7,6},{8,7},{9,8},{10,9... | collective-permute-start | bytes 1572872 | tf_op jit(solution)/shard_map/ppermute | solution.py:20
  335.5 8.6 %collective-permute-done = bf16[1024,256]{1,0:T(8,128)(2,1)S(1)} collective-permute-done((bf16[1024,256]{1,0:T(8,128)(2,1)S(1)}, bf16[1024,256]{1,0:T(8,128)(2,1)S(1)}, u32[]{:S(2)}, u32[]{:S(2)}) %collective-permute-start) | collective-permute-done | bytes 524320 | tf_op jit(solution)/shard_map/ppermute | solution.py:17
  344.1 1.9 collective-permute-start.2
  346.1 6.7 %collective-permute-start.3 = (bf16[1024,256]{1,0:T(8,128)(2,1)S(1)}, bf16[1024,256]{1,0:T(8,128)(2,1)S(1)}, u32[]{:S(2)}, u32[]{:S(2)}) collective-permute-start(bf16[1024,256]{1,0:T(8,128)(2,1)S(1)} %collective-permute-done.1), channel_id=1, source_target_pairs={{0,15},{1,0},{2,1},{3,2},{4,3},{5,4},{6,5},{7,6},{8,7},{9,8},{10,9... | collective-permute-start | bytes 1572872 | tf_op jit(solution)/shard_map/ppermute | solution.py:20
  352.8 7.7 %collective-permute-done.2 = bf16[1024,256]{1,0:T(8,128)(2,1)S(1)} collective-permute-done((bf16[1024,256]{1,0:T(8,128)(2,1)S(1)}, bf16[1024,256]{1,0:T(8,128)(2,1)S(1)}, u32[]{:S(2)}, u32[]{:S(2)}) %collective-permute-start.2) | collective-permute-done | bytes 524320 | tf_op jit(solution)/shard_map/ppermute | solution.py:17
  360.5 1.9 collective-permute-start.4
  362.4 6.7 %collective-permute-start.5 = (bf16[1024,256]{1,0:T(8,128)(2,1)S(1)}, bf16[1024,256]{1,0:T(8,128)(2,1)S(1)}, u32[]{:S(2)}, u32[]{:S(2)}) collective-permute-start(bf16[1024,256]{1,0:T(8,128)(2,1)S(1)} %collective-permute-done.3), channel_id=1, source_target_pairs={{0,15},{1,0},{2,1},{3,2},{4,3},{5,4},{6,5},{7,6},{8,7},{9,8},{10,9... | collective-permute-start | bytes 1572872 | tf_op jit(solution)/shard_map/ppermute | solution.py:20
  369.1 6.9 %collective-permute-done.4 = bf16[1024,256]{1,0:T(8,128)(2,1)S(1)} collective-permute-done((bf16[1024,256]{1,0:T(8,128)(2,1)S(1)}, bf16[1024,256]{1,0:T(8,128)(2,1)S(1)}, u32[]{:S(2)}, u32[]{:S(2)}) %collective-permute-start.4) | collective-permute-done | bytes 524320 | tf_op jit(solution)/shard_map/ppermute | solution.py:17
  376.8 1.9 collective-permute-start.6
  378.7 6.7 %collective-permute-start.7 = (bf16[1024,256]{1,0:T(8,128)(2,1)S(1)}, bf16[1024,256]{1,0:T(8,128)(2,1)}, u32[]{:S(2)}, u32[]{:S(2)}) collective-permute-start(bf16[1024,256]{1,0:T(8,128)(2,1)S(1)} %collective-permute-done.5), channel_id=1, source_target_pairs={{0,15},{1,0},{2,1},{3,2},{4,3},{5,4},{6,5},{7,6},{8,7},{9,8},{10,9... | collective-permute-start | bytes 1572872 | tf_op jit(solution)/shard_map/ppermute | solution.py:20
  385.4 6.0 %collective-permute-done.6 = bf16[1024,256]{1,0:T(8,128)(2,1)S(1)} collective-permute-done((bf16[1024,256]{1,0:T(8,128)(2,1)S(1)}, bf16[1024,256]{1,0:T(8,128)(2,1)S(1)}, u32[]{:S(2)}, u32[]{:S(2)}) %collective-permute-start.6) | collective-permute-done | bytes 524320 | tf_op jit(solution)/shard_map/ppermute | solution.py:17
  391.4 1.9 collective-permute-start.8
  393.4 6.7 %collective-permute-start.9 = (bf16[1024,256]{1,0:T(8,128)(2,1)}, bf16[1024,256]{1,0:T(8,128)(2,1)}, u32[]{:S(2)}, u32[]{:S(2)}) collective-permute-start(bf16[1024,256]{1,0:T(8,128)(2,1)} %collective-permute-done.7), channel_id=1, source_target_pairs={{0,15},{1,0},{2,1},{3,2},{4,3},{5,4},{6,5},{7,6},{8,7},{9,8},{10,9... | collective-permute-start | bytes 1572872 | tf_op jit(solution)/shard_map/ppermute | solution.py:20
  400.1 5.3 collective-permute-done.8
  405.3 1.9 collective-permute-start.10
  407.5 2.0 constant_dynamic-update-slice_fusion.14
  409.5 1.9 constant_dynamic-update-slice_fusion.13
  411.5 1.9 constant_dynamic-update-slice_fusion.12
  413.4 6.7 %collective-permute-start.11 = (bf16[1024,256]{1,0:T(8,128)(2,1)}, bf16[1024,256]{1,0:T(8,128)(2,1)S(1)}, u32[]{:S(2)}, u32[]{:S(2)}) collective-permute-start(bf16[1024,256]{1,0:T(8,128)(2,1)} %collective-permute-done.9), channel_id=1, source_target_pairs={{0,15},{1,0},{2,1},{3,2},{4,3},{5,4},{6,5},{7,6},{8,7},{9,8},{10,9... | collective-permute-start | bytes 1572872 | tf_op jit(solution)/shard_map/ppermute | solution.py:20
  420.1 2.0 constant_dynamic-update-slice_fusion.11
  422.0 1.9 collective-permute-start.12
  423.9 1.9 constant_dynamic-update-slice_fusion.10
  425.9 1.9 constant_dynamic-update-slice_fusion.9
  427.8 1.9 constant_dynamic-update-slice_fusion.8
  429.7 1.9 constant_dynamic-update-slice_fusion.7
  431.7 6.7 %collective-permute-start.13 = (bf16[1024,256]{1,0:T(8,128)(2,1)S(1)}, bf16[1024,256]{1,0:T(8,128)(2,1)S(1)}, u32[]{:S(2)}, u32[]{:S(2)}) collective-permute-start(bf16[1024,256]{1,0:T(8,128)(2,1)S(1)} %collective-permute-done.11), channel_id=1, source_target_pairs={{0,15},{1,0},{2,1},{3,2},{4,3},{5,4},{6,5},{7,6},{8,7},{9,8},{10,9... | collective-permute-start | bytes 1572872 | tf_op jit(solution)/shard_map/ppermute | solution.py:20
  438.4 1.9 constant_dynamic-update-slice_fusion.6
  440.3 2.1 collective-permute-start.14
  442.5 1.9 constant_dynamic-update-slice_fusion.5
  444.4 1.9 constant_dynamic-update-slice_fusion.4
  448.1 0.9 constant_dynamic-update-slice_fusion.1
  449.0 4.6 collective-permute-done.14
  454.4 6.4 %convolution_convert_fusion.1 = bf16[1024,128]{1,0:T(8,128)(2,1)} fusion(bf16[1024,4096]{1,0:T(8,128)(2,1)} %constant_dynamic-update-slice_fusion, bf16[1,4096,128]{2,1,0:T(8,128)(2,1)S(1)} %copy-done.13), kind=kOutput, calls=%fused_computation.53 | convolution fusion | flops 1073872896 | bytes 9699328 | tf_op jit(solution)/shard_map/dot_general | solution.py:211
  460.8 17.9 %all-to-all-start.4 = ((bf16[32,32,128]{2,1,0:T(8,128)(2,1)}), bf16[32,32,128]{2,1,0:T(8,128)(2,1)S(1)}, u32[]{:S(2)}, u32[]{:S(2)}) async-start(bf16[32,32,128]{2,1,0:T(8,128)(2,1)} %bitcast.155), calls=%async_computation.4 | async-start | bytes 524288 | tf_op jit(solution)/shard_map/all_to_all | solution.py:215
  479.6 21.4 %all-to-all-done.4 = bf16[32,32,128]{2,1,0:T(8,128)(2,1)S(1)} async-done(((bf16[32,32,128]{2,1,0:T(8,128)(2,1)}), bf16[32,32,128]{2,1,0:T(8,128)(2,1)S(1)}, u32[]{:S(2)}, u32[]{:S(2)}) %all-to-all-start.4) | async-done | bytes 262176 | tf_op jit(solution)/shard_map/all_to_all | solution.py:215
  501.0 1.9 gather_fusion.1
  502.9 1.4 fusion.40
  504.5 19.0 %all_to_all.31 = bf16[16,256,128]{2,1,0:T(8,128)(2,1)S(1)} all-to-all(bf16[16,256,128]{2,1,0:T(8,128)(2,1)S(1)} %broadcast_in_dim.71), channel_id=1, replica_groups=mesh['sp'=32,'tp'=16] {'tp'}, dimensions={0} | all-to-all | bytes 2097152 | tf_op jit(solution)/shard_map/all_to_all | solution.py:54
  523.5 1.5 fusion.30
  (159 shorter events, 19.6 us)
Async XLA Ops:
  6.5 318.2 %copy-start = (bf16[1,2048,256]{2,1,0:T(8,128)(2,1)S(1)}, bf16[1,2048,256]{2,1,0:T(8,128)(2,1)}, u32[]{:S(2)}) copy-start(bf16[1,2048,256]{2,1,0:T(8,128)(2,1)} %param.26) | copy-start | bytes 3145732
  6.5 82.2 %all-gather.2.cloned.1.call-start = ((), (), s32[]{:S(2)}) async-start(), calls=%async_computation.6 | async-start | bytes 4325376 | tf_op jit(solution)/shard_map/all_gather | solution.py:33
  92.6 33.2 %copy-start.11 = (f32[128]{0:T(128)S(1)}, f32[128]{0:T(128)}, u32[]{:S(2)}) copy-start(f32[128]{0:T(128)} %param.22) | copy-start | bytes 1540
  92.6 42.4 %copy-start.9 = (s32[256,2]{0,1:T(2,128)S(1)}, s32[256,2]{0,1:T(2,128)}, u32[]{:S(2)}) copy-start(s32[256,2]{0,1:T(2,128)} %param.28) | copy-start | bytes 6148
  125.8 47.3 %copy-start.1 = (bf16[256,2048]{1,0:T(8,128)(2,1)S(1)}, bf16[256,2048]{1,0:T(8,128)(2,1)}, u32[]{:S(2)}) copy-start(bf16[256,2048]{1,0:T(8,128)(2,1)} %param.17) | copy-start | bytes 3145732
  128.5 23.0 %all-to-all-start = ((bf16[16,16,2048]{2,1,0:T(8,128)(2,1)}), bf16[16,16,2048]{2,1,0:T(8,128)(2,1)S(1)}, u32[]{:S(2)}, u32[]{:S(2)}) async-start(bf16[16,16,2048]{2,1,0:T(8,128)(2,1)} %bitcast.147), calls=%async_computation | async-start | bytes 2097152 | tf_op jit(solution)/shard_map/all_to_all | solution.py:43
  152.7 20.4 %all-to-all-start.1 = ((bf16[16,16,2048]{2,1,0:T(8,128)(2,1)}), bf16[16,16,2048]{2,1,0:T(8,128)(2,1)S(1)}, u32[]{:S(2)}, u32[]{:S(2)}) async-start(bf16[16,16,2048]{2,1,0:T(8,128)(2,1)} %broadcast_in_dim.40), calls=%async_computation.1 | async-start | bytes 2097152 | tf_op jit(solution)/shard_map/all_to_all | solution.py:54
  244.8 67.2 %all-to-all-start.3 = ((bf16[16,32,32,128]{3,2,1,0:T(8,128)(2,1)}), bf16[16,32,32,128]{3,2,1,0:T(8,128)(2,1)}, u32[]{:S(2)}, u32[]{:S(2)}) async-start(bf16[16,32,32,128]{3,2,1,0:T(8,128)(2,1)} %broadcast_in_dim.70), calls=%async_computation.3 | async-start | bytes 8388608 | tf_op jit(solution)/shard_map/all_to_all | solution.py:54
  312.1 7.1 %copy-start.12 = (bf16[1,2048,256]{2,1,0:T(8,128)(2,1)S(1)}, bf16[1,2048,256]{2,1,0:T(8,128)(2,1)}, u32[]{:S(2)}) copy-start(bf16[1,2048,256]{2,1,0:T(8,128)(2,1)} %param.25) | copy-start | bytes 3145732
  326.9 17.2 %collective-permute-start = (bf16[1024,256]{1,0:T(8,128)(2,1)S(1)}, bf16[1024,256]{1,0:T(8,128)(2,1)S(1)}, u32[]{:S(2)}, u32[]{:S(2)}) collective-permute-start(bf16[1024,256]{1,0:T(8,128)(2,1)S(1)} %get-tuple-element.328), channel_id=1, source_target_pairs={{0,1},{1,2},{2,3},{3,4},{4,5},{5,6},{6,7},{7,8},{8,9},{9,10},{10,1... | collective-permute-start | bytes 1572872 | tf_op jit(solution)/shard_map/ppermute | solution.py:17
  328.8 17.2 %collective-permute-start.1 = (bf16[1024,256]{1,0:T(8,128)(2,1)S(1)}, bf16[1024,256]{1,0:T(8,128)(2,1)S(1)}, u32[]{:S(2)}, u32[]{:S(2)}) collective-permute-start(bf16[1024,256]{1,0:T(8,128)(2,1)S(1)} %get-tuple-element.328), channel_id=1, source_target_pairs={{0,15},{1,0},{2,1},{3,2},{4,3},{5,4},{6,5},{7,6},{8,7},{9,8},{10,9... | collective-permute-start | bytes 1572872 | tf_op jit(solution)/shard_map/ppermute | solution.py:20
  344.1 8.6 %copy-start.3 = (bf16[1024,256]{1,0:T(8,128)(2,1)}, bf16[1024,256]{1,0:T(8,128)(2,1)S(1)}, u32[]{:S(2)}) copy-start(bf16[1024,256]{1,0:T(8,128)(2,1)S(1)} %collective-permute-done) | copy-start | bytes 1572868
  344.1 16.4 %collective-permute-start.2 = (bf16[1024,256]{1,0:T(8,128)(2,1)S(1)}, bf16[1024,256]{1,0:T(8,128)(2,1)S(1)}, u32[]{:S(2)}, u32[]{:S(2)}) collective-permute-start(bf16[1024,256]{1,0:T(8,128)(2,1)S(1)} %collective-permute-done), channel_id=1, source_target_pairs={{0,1},{1,2},{2,3},{3,4},{4,5},{5,6},{6,7},{7,8},{8,9},{9,10},{10,1... | collective-permute-start | bytes 1572872 | tf_op jit(solution)/shard_map/ppermute | solution.py:17
  346.1 16.3 %copy-start.5 = (bf16[1024,256]{1,0:T(8,128)(2,1)}, bf16[1024,256]{1,0:T(8,128)(2,1)S(1)}, u32[]{:S(2)}) copy-start(bf16[1024,256]{1,0:T(8,128)(2,1)S(1)} %collective-permute-done.1) | copy-start | bytes 1572868
  346.1 16.3 %collective-permute-start.3 = (bf16[1024,256]{1,0:T(8,128)(2,1)S(1)}, bf16[1024,256]{1,0:T(8,128)(2,1)S(1)}, u32[]{:S(2)}, u32[]{:S(2)}) collective-permute-start(bf16[1024,256]{1,0:T(8,128)(2,1)S(1)} %collective-permute-done.1), channel_id=1, source_target_pairs={{0,15},{1,0},{2,1},{3,2},{4,3},{5,4},{6,5},{7,6},{8,7},{9,8},{10,9... | collective-permute-start | bytes 1572872 | tf_op jit(solution)/shard_map/ppermute | solution.py:20
  360.5 8.6 %copy-start.8 = (bf16[1024,256]{1,0:T(8,128)(2,1)}, bf16[1024,256]{1,0:T(8,128)(2,1)S(1)}, u32[]{:S(2)}) copy-start(bf16[1024,256]{1,0:T(8,128)(2,1)S(1)} %collective-permute-done.2) | copy-start | bytes 1572868
  360.5 15.5 %collective-permute-start.4 = (bf16[1024,256]{1,0:T(8,128)(2,1)S(1)}, bf16[1024,256]{1,0:T(8,128)(2,1)S(1)}, u32[]{:S(2)}, u32[]{:S(2)}) collective-permute-start(bf16[1024,256]{1,0:T(8,128)(2,1)S(1)} %collective-permute-done.2), channel_id=1, source_target_pairs={{0,1},{1,2},{2,3},{3,4},{4,5},{5,6},{6,7},{7,8},{8,9},{9,10},{10,1... | collective-permute-start | bytes 1572872 | tf_op jit(solution)/shard_map/ppermute | solution.py:17
  362.4 30.9 %copy-start.6 = (bf16[1024,256]{1,0:T(8,128)(2,1)}, bf16[1024,256]{1,0:T(8,128)(2,1)S(1)}, u32[]{:S(2)}) copy-start(bf16[1024,256]{1,0:T(8,128)(2,1)S(1)} %collective-permute-done.3) | copy-start | bytes 1572868
  362.4 16.3 %collective-permute-start.5 = (bf16[1024,256]{1,0:T(8,128)(2,1)S(1)}, bf16[1024,256]{1,0:T(8,128)(2,1)S(1)}, u32[]{:S(2)}, u32[]{:S(2)}) collective-permute-start(bf16[1024,256]{1,0:T(8,128)(2,1)S(1)} %collective-permute-done.3), channel_id=1, source_target_pairs={{0,15},{1,0},{2,1},{3,2},{4,3},{5,4},{6,5},{7,6},{8,7},{9,8},{10,9... | collective-permute-start | bytes 1572872 | tf_op jit(solution)/shard_map/ppermute | solution.py:20
  376.0 0.8 copy-start.2
  376.8 14.6 %collective-permute-start.6 = (bf16[1024,256]{1,0:T(8,128)(2,1)S(1)}, bf16[1024,256]{1,0:T(8,128)(2,1)S(1)}, u32[]{:S(2)}, u32[]{:S(2)}) collective-permute-start(bf16[1024,256]{1,0:T(8,128)(2,1)S(1)} %collective-permute-done.4), channel_id=1, source_target_pairs={{0,1},{1,2},{2,3},{3,4},{4,5},{5,6},{6,7},{7,8},{8,9},{9,10},{10,1... | collective-permute-start | bytes 1572872 | tf_op jit(solution)/shard_map/ppermute | solution.py:17
  378.7 12.7 %copy-start.4 = (bf16[1024,256]{1,0:T(8,128)(2,1)}, bf16[1024,256]{1,0:T(8,128)(2,1)S(1)}, u32[]{:S(2)}) copy-start(bf16[1024,256]{1,0:T(8,128)(2,1)S(1)} %collective-permute-done.5) | copy-start | bytes 1572868
  378.7 14.6 %collective-permute-start.7 = (bf16[1024,256]{1,0:T(8,128)(2,1)S(1)}, bf16[1024,256]{1,0:T(8,128)(2,1)}, u32[]{:S(2)}, u32[]{:S(2)}) collective-permute-start(bf16[1024,256]{1,0:T(8,128)(2,1)S(1)} %collective-permute-done.5), channel_id=1, source_target_pairs={{0,15},{1,0},{2,1},{3,2},{4,3},{5,4},{6,5},{7,6},{8,7},{9,8},{10,9... | collective-permute-start | bytes 1572872 | tf_op jit(solution)/shard_map/ppermute | solution.py:20
  391.4 8.6 %copy-start.7 = (bf16[1024,256]{1,0:T(8,128)(2,1)}, bf16[1024,256]{1,0:T(8,128)(2,1)S(1)}, u32[]{:S(2)}) copy-start(bf16[1024,256]{1,0:T(8,128)(2,1)S(1)} %collective-permute-done.6) | copy-start | bytes 1572868
  391.4 13.9 %collective-permute-start.8 = (bf16[1024,256]{1,0:T(8,128)(2,1)S(1)}, bf16[1024,256]{1,0:T(8,128)(2,1)}, u32[]{:S(2)}, u32[]{:S(2)}) collective-permute-start(bf16[1024,256]{1,0:T(8,128)(2,1)S(1)} %collective-permute-done.6), channel_id=1, source_target_pairs={{0,1},{1,2},{2,3},{3,4},{4,5},{5,6},{6,7},{7,8},{8,9},{9,10},{10,1... | collective-permute-start | bytes 1572872 | tf_op jit(solution)/shard_map/ppermute | solution.py:17
  393.4 20.0 %collective-permute-start.9 = (bf16[1024,256]{1,0:T(8,128)(2,1)}, bf16[1024,256]{1,0:T(8,128)(2,1)}, u32[]{:S(2)}, u32[]{:S(2)}) collective-permute-start(bf16[1024,256]{1,0:T(8,128)(2,1)} %collective-permute-done.7), channel_id=1, source_target_pairs={{0,15},{1,0},{2,1},{3,2},{4,3},{5,4},{6,5},{7,6},{8,7},{9,8},{10,9... | collective-permute-start | bytes 1572872 | tf_op jit(solution)/shard_map/ppermute | solution.py:20
  405.3 16.7 %collective-permute-start.10 = (bf16[1024,256]{1,0:T(8,128)(2,1)}, bf16[1024,256]{1,0:T(8,128)(2,1)}, u32[]{:S(2)}, u32[]{:S(2)}) collective-permute-start(bf16[1024,256]{1,0:T(8,128)(2,1)} %collective-permute-done.8), channel_id=1, source_target_pairs={{0,1},{1,2},{2,3},{3,4},{4,5},{5,6},{6,7},{7,8},{8,9},{9,10},{10,1... | collective-permute-start | bytes 1572872 | tf_op jit(solution)/shard_map/ppermute | solution.py:17
  407.5 46.9 %copy-start.13 = (bf16[1,4096,128]{2,1,0:T(8,128)(2,1)S(1)}, bf16[1,4096,128]{2,1,0:T(8,128)(2,1)}, u32[]{:S(2)}) copy-start(bf16[1,4096,128]{2,1,0:T(8,128)(2,1)} %param.27) | copy-start | bytes 3145732
  413.4 18.3 %collective-permute-start.11 = (bf16[1024,256]{1,0:T(8,128)(2,1)}, bf16[1024,256]{1,0:T(8,128)(2,1)S(1)}, u32[]{:S(2)}, u32[]{:S(2)}) collective-permute-start(bf16[1024,256]{1,0:T(8,128)(2,1)} %collective-permute-done.9), channel_id=1, source_target_pairs={{0,15},{1,0},{2,1},{3,2},{4,3},{5,4},{6,5},{7,6},{8,7},{9,8},{10,9... | collective-permute-start | bytes 1572872 | tf_op jit(solution)/shard_map/ppermute | solution.py:20
  422.0 18.3 %collective-permute-start.12 = (bf16[1024,256]{1,0:T(8,128)(2,1)}, bf16[1024,256]{1,0:T(8,128)(2,1)S(1)}, u32[]{:S(2)}, u32[]{:S(2)}) collective-permute-start(bf16[1024,256]{1,0:T(8,128)(2,1)} %collective-permute-done.10), channel_id=1, source_target_pairs={{0,1},{1,2},{2,3},{3,4},{4,5},{5,6},{6,7},{7,8},{8,9},{9,10},{10,1... | collective-permute-start | bytes 1572872 | tf_op jit(solution)/shard_map/ppermute | solution.py:17
  431.7 16.4 %collective-permute-start.13 = (bf16[1024,256]{1,0:T(8,128)(2,1)S(1)}, bf16[1024,256]{1,0:T(8,128)(2,1)S(1)}, u32[]{:S(2)}, u32[]{:S(2)}) collective-permute-start(bf16[1024,256]{1,0:T(8,128)(2,1)S(1)} %collective-permute-done.11), channel_id=1, source_target_pairs={{0,15},{1,0},{2,1},{3,2},{4,3},{5,4},{6,5},{7,6},{8,7},{9,8},{10,9... | collective-permute-start | bytes 1572872 | tf_op jit(solution)/shard_map/ppermute | solution.py:20
  440.3 13.2 %collective-permute-start.14 = (bf16[1024,256]{1,0:T(8,128)(2,1)S(1)}, bf16[1024,256]{1,0:T(8,128)(2,1)S(1)}, u32[]{:S(2)}, u32[]{:S(2)}) collective-permute-start(bf16[1024,256]{1,0:T(8,128)(2,1)S(1)} %collective-permute-done.12), channel_id=1, source_target_pairs={{0,1},{1,2},{2,3},{3,4},{4,5},{5,6},{6,7},{7,8},{8,9},{9,10},{10,1... | collective-permute-start | bytes 1572872 | tf_op jit(solution)/shard_map/ppermute | solution.py:17
  446.3 32.5 %copy-start.10 = (f32[256,2]{0,1:T(2,128)S(1)}, f32[256,2]{0,1:T(2,128)}, u32[]{:S(2)}) copy-start(f32[256,2]{0,1:T(2,128)} %param.29) | copy-start | bytes 6148
  460.8 40.2 %all-to-all-start.4 = ((bf16[32,32,128]{2,1,0:T(8,128)(2,1)}), bf16[32,32,128]{2,1,0:T(8,128)(2,1)S(1)}, u32[]{:S(2)}, u32[]{:S(2)}) async-start(bf16[32,32,128]{2,1,0:T(8,128)(2,1)} %bitcast.155), calls=%async_computation.4 | async-start | bytes 524288 | tf_op jit(solution)/shard_map/all_to_all | solution.py:215
Sparse Core Ops, SparseCore 0:
  9.5 79.1 all-gather.1
